TPU v7x, 32 devices: a whole 2x2x4 slice. The times are simulated.
32 devices in a mesh: ep: 16 (over z, y, core), tp: 2 (over x).
Axes of the slice: x: 2, y: 2, z: 4, core: 2. Of those that a mesh axis runs over, the one named last changes fastest.
Arguments:
- tokens: bfloat16 [256, 2048], P('ep'), may hold values from -6 to 6
- positions: int32 [256], P('ep'), may hold values from 1024 to 16383
- state: float32 [256, 4, 128, 128], P('ep', 'tp'), may hold values from -1 to 1
- mix_gain: float32 [2048], replicated, may hold values from 0.1 to 1.9
- w_query: bfloat16 [2048, 512], P(None, 'tp'), may hold values from -0.125 to 0.125
- w_key: bfloat16 [2048, 512], P(None, 'tp'), may hold values from -0.125 to 0.125
- w_value: bfloat16 [2048, 512], P(None, 'tp'), may hold values from -0.125 to 0.125
- w_out: bfloat16 [512, 2048], P('tp'), may hold values from -0.25 to 0.25
- ffn_gain: float32 [2048], replicated, may hold values from 0.1 to 1.9
- branch_gate: bfloat16 [2048], replicated, may hold values from -0.125 to 0.125
- dense_gate: bfloat16 [2048, 4096], P('tp', 'ep'), may hold values from -0.125 to 0.125
- dense_up: bfloat16 [2048, 4096], P('tp', 'ep'), may hold values from -0.125 to 0.125
- dense_down: bfloat16 [4096, 2048], P('ep', 'tp'), may hold values from -0.09375 to 0.09375
- routes: int32 [256, 6], P('ep'), may hold values from 0 to 15, all different within a row; in each aligned block of 16 rows (0 to 15, 16 to 31, ...) at most 12 rows name the same one
- route_scores: float32 [256, 6], P('ep'), may hold values from 0.05 to 1
- expert_gate: bfloat16 [16, 2048, 512], P('ep', None, 'tp'), may hold values from -0.125 to 0.125
- expert_up: bfloat16 [16, 2048, 512], P('ep', None, 'tp'), may hold values from -0.125 to 0.125
- expert_down: bfloat16 [16, 512, 2048], P('ep', 'tp'), may hold values from -0.25 to 0.25
Outputs:
- layer_out: bfloat16 [256, 2048], P('ep', 'tp')
Inputs may be any that keep to these rules, and one draw needn't show every extreme that they name: `routes`: each row names 6 different experts. In each aligned block of 16 rows (the rows of one index of ep) no expert is named by more than 12 rows, a bound that some block reaches.
All inputs are finite; a program needn't handle non-finite values.
Results may differ from a plain program's by a relative error of at most 0.012.
Values may be sent and summed in bfloat16 or wider, within the bound.
No kernel may reach another device: no remote copies, remote signals or barrier semaphores. Data moves between devices by JAX's collectives and lax.ppermute only.
A program may use at most 64 MiB of HBM per device.

v0:
```python
import jax
import jax.numpy as jnp
import numpy as np
from jax import lax
from jax.experimental import pallas as pl
from jax.experimental.pallas import tpu as pltpu
from jax.sharding import PartitionSpec as P

EPS = 1e-06
LANES = 128
F32 = jnp.float32
BF16 = jnp.bfloat16


def dot(a, b):
    return jnp.dot(a, b, preferred_element_type=F32)


def frequencies(head_dim):
    half = head_dim // 2
    inverse = 1.0 / 10000.0 ** np.linspace(0.0, 1.0, half)
    return jnp.asarray(np.concatenate([inverse, inverse])[None, :], F32)


def turns(angle):
    whole = jnp.round(angle * (0.5 / np.pi))
    first = 6.28125
    second = float(np.float32(2 * np.pi - first).astype(jnp.bfloat16))
    third = 2 * np.pi - first - second
    rest = ((angle - whole * first) - whole * second) - whole * third
    return jnp.cos(rest), jnp.sin(rest)


def mixer_kernel(tok, gain, where, freq, wq, wk, wv, st, wo, out, q_buf, k_buf, v_buf, s_buf, o_buf, sems):
    copies = [
        pltpu.make_async_copy(src, dst, sems.at[i])
        for i, (src, dst) in enumerate(
            [(wq, q_buf), (wk, k_buf), (wv, v_buf), (st, s_buf), (wo, o_buf)]
        )
    ]
    for copy in copies:
        copy.start()
    rows, heads, head_dim = s_buf.shape[0], s_buf.shape[1], s_buf.shape[2]
    values = tok[...].astype(F32)
    scale = lax.rsqrt(jnp.mean(values * values, axis=-1, keepdims=True) + EPS)
    normed = (values * scale * gain[...]).astype(BF16)
    copies[0].wait()
    query = dot(normed, q_buf[...])
    copies[1].wait()
    key = dot(normed, k_buf[...])
    copies[2].wait()
    value = dot(normed, v_buf[...])
    half = head_dim // 2
    square = (rows, rows)
    diagonal = lax.broadcasted_iota(jnp.int32, square, 0) == lax.broadcasted_iota(
        jnp.int32, square, 1
    )
    spread = jnp.broadcast_to(where[...].astype(F32), square)
    at = jnp.sum(jnp.where(diagonal, spread, 0.0), axis=1, keepdims=True)
    cosine, sine = turns(at * freq[...])
    sine = jnp.where(lax.broadcasted_iota(jnp.int32, sine.shape, 1) < half, -sine, sine)
    all_heads = heads * lax.axis_size("tp")
    first_head = lax.axis_index("tp") * heads
    copies[3].wait()
    parts = []
    for h in range(heads):
        cols = slice(h * head_dim, (h + 1) * head_dim)
        q = query[:, cols]
        k = key[:, cols]
        q = q * cosine + pltpu.roll(q, half, 1) * sine
        k = (k * cosine + pltpu.roll(k, half, 1) * sine) * head_dim ** (-0.5)
        turned = q.T
        old = jnp.concatenate(
            [
                jnp.sum(turned[:, b : b + 1] * s_buf[b, h], axis=0, keepdims=True)
                for b in range(rows)
            ],
            axis=0,
        )
        number = jnp.full((1, head_dim), first_head + h, jnp.int32).astype(F32)
        decay = 1.0 - jnp.exp2(-5.0 - 5.0 * number / (all_heads - 1))
        got = decay * old + jnp.sum(q * k, axis=-1, keepdims=True) * value[:, cols]
        got = got * lax.rsqrt(jnp.mean(got * got, axis=-1, keepdims=True) + EPS)
        parts.append(got.astype(BF16))
    retrieved = parts[0] if heads == 1 else jnp.concatenate(parts, axis=1)
    copies[4].wait()
    out[...] = dot(retrieved, o_buf[...]).astype(BF16)


def mixer(tokens, gain, positions, freq, wq, wk, wv, state, wo):
    vmem = pl.BlockSpec(memory_space=pltpu.VMEM)
    hbm = pl.BlockSpec(memory_space=pl.ANY)
    return pl.pallas_call(
        mixer_kernel,
        out_shape=jax.ShapeDtypeStruct(tokens.shape, BF16),
        in_specs=[vmem] * 4 + [hbm] * 5,
        out_specs=vmem,
        scratch_shapes=[pltpu.VMEM(a.shape, a.dtype) for a in (wq, wk, wv, state, wo)]
        + [pltpu.SemaphoreType.DMA((5,))],
        name="mixer",
    )(tokens, gain, positions, freq, wq, wk, wv, state, wo)


def norm_kernel(fanout, tok, gain, gate, meta, *refs):
    parts, (rows_out, mix_out) = refs[:-2], refs[-2:]
    width = tok.shape[1]
    mixed = parts[0][...].astype(F32)
    for part in parts[1:]:
        mixed = mixed + part[...].astype(F32)
    after = tok[...].astype(F32) + mixed
    mix_out[...] = after
    scale = lax.rsqrt(jnp.mean(after * after, axis=-1, keepdims=True) + EPS)
    ffn = (after * scale * gain[...]).astype(BF16)
    rows_out[:, :width] = ffn
    logit = jnp.sum(ffn.astype(F32) * gate[...].astype(F32), axis=-1, keepdims=True)
    branch = 1.0 / (1.0 + jnp.exp(-logit))
    high = branch.astype(BF16).astype(F32)
    low = branch - high
    info = meta[...].astype(F32)
    lane = lax.broadcasted_iota(jnp.int32, info.shape, 1)
    info = jnp.where(lane == 3 * fanout, high, info)
    info = jnp.where(lane == 3 * fanout + 1, low, info)
    rows_out[:, width:] = info.astype(BF16)


def norm_rows(fanout, tokens, gain, gate, meta, parts):
    vmem = pl.BlockSpec(memory_space=pltpu.VMEM)
    rows, width = tokens.shape
    return pl.pallas_call(
        lambda *refs: norm_kernel(fanout, *refs),
        out_shape=(
            jax.ShapeDtypeStruct((rows, width + LANES), BF16),
            jax.ShapeDtypeStruct((rows, width), F32),
        ),
        in_specs=[vmem] * (4 + len(parts)),
        out_specs=(vmem, vmem),
        name="norm",
    )(tokens, gain, gate, meta, *parts)


def silu(v):
    return v / (1.0 + jnp.exp(-v))


def branch_kernel(tp_count, fanout, near, far, eg, eu, ed, *refs):
    pieces = refs[: 2 * tp_count]
    near_out, far_out = refs[2 * tp_count : 2 * tp_count + 2]
    bufs = refs[2 * tp_count + 2 : -1]
    sems = refs[-1]
    sources = [eg, eu, *pieces[:tp_count], ed, *pieces[tp_count:]]
    copies = [
        pltpu.make_async_copy(src, dst, sems.at[i])
        for i, (src, dst) in enumerate(zip(sources, bufs))
    ]
    for copy in copies:
        copy.start()
    eg_buf, eu_buf = bufs[0], bufs[1]
    dg_bufs = bufs[2 : 2 + tp_count]
    ed_buf = bufs[2 + tp_count]
    dd_bufs = bufs[3 + tp_count :]
    width = eg_buf.shape[1]
    block = width // tp_count
    units = dd_bufs[0].shape[0]
    per_device = eg_buf.shape[0]
    ep_index = lax.axis_index("ep")
    tp_index = lax.axis_index("tp")
    spots = [lax.rem(tp_index - t + tp_count, tp_count) * block for t in range(tp_count)]
    spots = [pl.multiple_of(s, LANES) for s in spots]
    rows = near.shape[0]
    step = min(rows, 256)
    held = list(copies)

    def need(count):
        while len(copies) - len(held) < count:
            held.pop(0).wait()

    if rows != step:
        need(len(copies))

    def work(src, dst, start):
        at = pl.ds(start, step)
        info = src[at, width:].astype(F32)
        lane = lax.broadcasted_iota(jnp.int32, info.shape, 1)
        high = pltpu.roll(info, LANES - fanout, 1)
        low = pltpu.roll(info, LANES - 2 * fanout, 1)
        branch = jnp.sum(
            jnp.where((lane >= 3 * fanout) & (lane < 3 * fanout + 2), info, 0.0),
            axis=1,
            keepdims=True,
        )
        x = src[at, :width]
        hidden = []
        for k in range(per_device):
            own = (ep_index * per_device + k).astype(F32)
            weight = jnp.sum(
                jnp.where((lane < fanout) & (info == own), high + low, 0.0), axis=1, keepdims=True
            )
            need(1)
            gate = dot(x, eg_buf[k])
            need(2)
            hidden.append((silu(gate) * dot(x, eu_buf[k]) * weight).astype(BF16))
        need(2 + tp_count)
        both = dot(src[at, pl.ds(spots[0], block)], dg_bufs[0][...])
        for t in range(1, tp_count):
            both = both + dot(src[at, pl.ds(spots[t], block)], dg_bufs[t][...])
        dense = (silu(both[:, :units]) * both[:, units:] * branch).astype(BF16)
        need(len(copies))
        for t in range(tp_count):
            total = dot(dense, dd_bufs[t][...])
            for k in range(per_device):
                total = total + dot(hidden[k], ed_buf[k, :, pl.ds(spots[t], block)])
            dst[t, at, :] = total.astype(BF16)

    for src, dst in ((far, far_out), (near, near_out)):
        if rows == step:
            work(src, dst, 0)
        else:

            def body(i, carry, src=src, dst=dst):
                work(src, dst, pl.multiple_of(i * step, step))
                return carry

            lax.fori_loop(0, rows // step, body, 0)


def branches(fanout, near, far, eg, eu, ed, gate_pieces, down_pieces):
    vmem = pl.BlockSpec(memory_space=pltpu.VMEM)
    hbm = pl.BlockSpec(memory_space=pl.ANY)
    tp_count = len(gate_pieces)
    width = eg.shape[1]
    shape = jax.ShapeDtypeStruct((tp_count, near.shape[0], width // tp_count), BF16)
    order = [eg, eu, *gate_pieces, ed, *down_pieces]
    return pl.pallas_call(
        lambda *refs: branch_kernel(tp_count, fanout, *refs),
        out_shape=(shape, shape),
        in_specs=[vmem, vmem]
        + [hbm] * (3 + 2 * tp_count),
        out_specs=(vmem, vmem),
        scratch_shapes=[pltpu.VMEM(a.shape, a.dtype) for a in order]
        + [pltpu.SemaphoreType.DMA((len(order),))],
        name="branches",
    )(near, far, eg, eu, ed, *gate_pieces, *down_pieces)


def on_device(
    tokens,
    positions,
    state,
    mix_gain,
    w_query,
    w_key,
    w_value,
    w_out,
    ffn_gain,
    branch_gate,
    dense_gate,
    dense_up,
    dense_down,
    routes,
    route_scores,
    expert_gate,
    expert_up,
    expert_down,
):
    sequences, width = tokens.shape
    tp_count = lax.axis_size("tp")
    ep_count = lax.axis_size("ep")
    tp_index = lax.axis_index("tp")
    fanout = routes.shape[1]
    block = width // tp_count
    cores = 2 if ep_count % 2 == 0 else 1
    chips = ep_count // cores
    y_count = 1
    while chips % (y_count * 2) == 0 and (y_count * 2) ** 2 <= chips:
        y_count *= 2
    z_count = chips // y_count

    def send(x, dz=0, dy=0, dc=0, dx=0):
        pairs = []
        for z in range(z_count):
            for y in range(y_count):
                for c in range(cores):
                    for q in range(tp_count):
                        src = ((z * y_count + y) * cores + c) * tp_count + q
                        to_z, to_y = (z + dz) % z_count, (y + dy) % y_count
                        to_c, to_q = (c + dc) % cores, (q + dx) % tp_count
                        dst = ((to_z * y_count + to_y) * cores + to_c) * tp_count + to_q
                        pairs.append((src, dst))
        return lax.ppermute(x, ("ep", "tp"), pairs)

    partial_out = mixer(
        tokens,
        mix_gain[None, :],
        positions[None, :],
        frequencies(state.shape[2]),
        w_query,
        w_key,
        w_value,
        state,
        w_out,
    )
    parts = [partial_out] + [send(partial_out, dx=s) for s in range(1, tp_count)]

    route_weights = route_scores / jnp.sum(route_scores, axis=1, keepdims=True)
    high = lax.reduce_precision(route_weights, 8, 7)
    low = route_weights - high
    meta = jnp.concatenate([routes.astype(F32), high, low], axis=1)
    meta = jnp.pad(meta, ((0, 0), (0, LANES - meta.shape[1]))).astype(BF16)
    payload, after_mix = norm_rows(
        fanout, tokens, ffn_gain[None, :], branch_gate[None, :], meta, parts
    )

    units = dense_gate.shape[1] // tp_count

    def gate_piece(index):
        at = lax.rem(index, tp_count) * units
        return jnp.concatenate(
            [
                lax.dynamic_slice_in_dim(dense_gate, at, units, 1),
                lax.dynamic_slice_in_dim(dense_up, at, units, 1),
            ],
            axis=1,
        )

    def down_piece(index):
        return lax.dynamic_slice_in_dim(dense_down, lax.rem(index, tp_count) * units, units, 0)

    gate_pieces = [gate_piece(tp_index)]
    down_pieces = [down_piece(tp_index)]
    for s in range(1, tp_count):
        there_gate, there_down, _ = lax.optimization_barrier(
            (gate_piece(tp_index + s), down_piece(tp_index + s), parts[s])
        )
        gate_pieces.append(send(there_gate, dx=s))
        down_pieces.append(send(there_down, dx=s))

    rows = jnp.concatenate([payload] + [send(payload, dz=s) for s in range(1, z_count)], axis=0)
    rows = jnp.concatenate([rows] + [send(rows, dy=s) for s in range(1, y_count)], axis=0)
    if cores == 2:
        far = send(rows, dc=1)
    else:
        far = rows
    near_sum, far_sum = branches(
        fanout, rows, far, expert_gate, expert_up, expert_down, gate_pieces, down_pieces
    )

    total = near_sum.astype(F32)
    if cores == 2:
        total = total + send(far_sum, dc=1).astype(F32)
    total = total.reshape(tp_count, y_count, z_count * sequences, block)
    narrow = total.astype(BF16)
    summed = total[0, 0]
    for t in range(tp_count):
        for y in range(y_count):
            if (t, y) != (0, 0):
                summed = summed + send(narrow[t, y], dx=-t, dy=-y).astype(F32)
    summed = summed.reshape(z_count, sequences, block)
    narrow = summed.astype(BF16)
    result = lax.dynamic_slice_in_dim(after_mix, tp_index * block, block, 1) + summed[0]
    for z in range(1, z_count):
        result = result + send(narrow[z], dz=-z).astype(F32)
    return result.astype(BF16)


def solution(mesh):
    placed = (
        P("ep", None),
        P("ep"),
        P("ep", "tp", None, None),
        P(),
        P(None, "tp"),
        P(None, "tp"),
        P(None, "tp"),
        P("tp", None),
        P(),
        P(),
        P("tp", "ep"),
        P("tp", "ep"),
        P("ep", "tp"),
        P("ep", None),
        P("ep", None),
        P("ep", None, "tp"),
        P("ep", None, "tp"),
        P("ep", "tp", None),
    )

    return jax.shard_map(
        on_device, mesh=mesh, in_specs=placed, out_specs=P("ep", "tp"), check_vma=False
    )
```

profile of v0, /device:TPU:0, one launch (start us, length us, event | category | flops | bytes accessed | tf_op | source)
XLA Modules:
  0.0 81.3 jit_solution(12277813569861016668)
XLA Ops:
  0.0 5.9 %mixer.1.refs_4_ = bf16[16,2048]{1,0:T(8,128)(2,1)} custom-call(bf16[16,2048]{1,0:T(8,128)(2,1)} %refs_0_.1, f32[1,2048]{1,0:T(1,128)} %bitcast.21, s32[1,16]{1,0:T(1,128)} %bitcast.23, f32[1,128]{1,0:T(1,128)} %constant.28.clone.freq, bf16[2048,256]{1,0:T(8,128)(2,1)} %wq.1, bf16[2048,256]{1,0:T(8,128)(2,1)} %wk.1, bf16[2048,256]{1,0:T(8,128)(2,1)} %wv.1, ...), custom_call_target="tpu_custom_call" | custom-call | tf_op jit(solution)/shard_map/mixer/pallas_call | solution.py:93
  5.9 3.0 %collective-permute-start = (bf16[16,2048]{1,0:T(8,128)(2,1)}, bf16[16,2048]{1,0:T(8,128)(2,1)S(1)}, u32[]{:S(2)}, u32[]{:S(2)}) collective-permute-start(bf16[16,2048]{1,0:T(8,128)(2,1)} %mixer.1.refs_4_), channel_id=1, source_target_pairs={{0,1},{1,0},{2,3},{3,2},{4,5},{5,4},{6,7},{7,6},{8,9},{9,8},{10,11... | collective-permute-start | bytes 196616 | tf_op jit(solution)/shard_map/ppermute | solution.py:289
  8.9 0.1 copy.23
  9.1 0.1 copy.22
  9.2 0.6 broadcast_in_dim.14.refs_2_
  9.8 0.1 reduce-precision_convert_fusion
  9.9 0.7 constant_dynamic-slice_fusion
  10.6 0.2 constant_dynamic-slice_fusion.2
  10.8 0.7 fusion.12.refs_3_
  11.4 0.0 collective-permute-done.refs_5_
  11.5 0.6 copy-done.7
  12.1 1.8 %norm.1 = (bf16[16,2176]{1,0:T(8,128)(2,1)}, f32[16,2048]{1,0:T(8,128)}) custom-call(bf16[16,2048]{1,0:T(8,128)(2,1)} %refs_0_.1, f32[1,2048]{1,0:T(1,128)} %bitcast.22, bf16[1,2048]{1,0:T(2,128)(2,1)} %broadcast_in_dim.14.refs_2_, bf16[16,128]{1,0:T(8,128)(2,1)} %fusion.12.refs_3_, bf16[16,2048]{1,0:T(8,128)(2,1)} %mixer.1.refs_4_, bf16[16,2048]{1,0:T(8,128)(2,1)} %copy-done.7), custom_call_target="tpu_custom_call" | custom-call | tf_op jit(solution)/shard_map/norm/pallas_call | solution.py:129
  13.9 4.1 %collective-permute-start.3 = (bf16[16,2176]{1,0:T(8,128)(2,1)}, bf16[16,2176]{1,0:T(8,128)(2,1)S(1)}, u32[]{:S(2)}, u32[]{:S(2)}) collective-permute-start(bf16[16,2176]{1,0:T(8,128)(2,1)} %get-tuple-element.12), channel_id=1, source_target_pairs={{0,24},{1,25},{2,26},{3,27},{4,28},{5,29},{6,30},{7,31},{8,0},{9,1... | collective-permute-start | bytes 208904 | tf_op jit(solution)/shard_map/ppermute | solution.py:289
  18.0 1.0 %collective-permute-start.1 = (bf16[16,2176]{1,0:T(8,128)(2,1)}, bf16[16,2176]{1,0:T(8,128)(2,1)S(1)}, u32[]{:S(2)}, u32[]{:S(2)}) collective-permute-start(bf16[16,2176]{1,0:T(8,128)(2,1)} %get-tuple-element.12), channel_id=1, source_target_pairs={{0,8},{1,9},{2,10},{3,11},{4,12},{5,13},{6,14},{7,15},{8,16},{9,17... | collective-permute-start | bytes 208904 | tf_op jit(solution)/shard_map/ppermute | solution.py:289
  19.0 0.9 %constant_dynamic-update-slice_fusion.4 = bf16[128,2176]{1,0:T(8,128)(2,1)S(1)} fusion(bf16[16,2176]{1,0:T(8,128)(2,1)} %get-tuple-element.12), kind=kLoop, calls=%fused_computation.20 | loop fusion | bytes 139264
  19.9 0.6 collective-permute-done.3
  20.5 3.0 %collective-permute-done.2 = bf16[16,2176]{1,0:T(8,128)(2,1)S(1)} collective-permute-done((bf16[16,2176]{1,0:T(8,128)(2,1)}, bf16[16,2176]{1,0:T(8,128)(2,1)S(1)}, u32[]{:S(2)}, u32[]{:S(2)}) %collective-permute-start.2) | collective-permute-done | bytes 69664 | tf_op jit(solution)/shard_map/ppermute | solution.py:289
  23.5 0.8 collective-permute-done.1
  24.3 0.9 %pad_maximum_fusion.2 = bf16[64,2176]{1,0:T(8,128)(2,1)S(1)} fusion(bf16[16,2176]{1,0:T(8,128)(2,1)S(1)} %collective-permute-done.3, bf16[16,2176]{1,0:T(8,128)(2,1)S(1)} %collective-permute-done.2, bf16[16,2176]{1,0:T(8,128)(2,1)S(1)} %collective-permute-done.1, bf16[16,2176]{1,0:T(8,128)(2,1)} %get-tuple-element.12), kind=kLoop, calls=%fused_computation.3 | loop fusion | flops 1114112 | bytes 557056 | tf_op jit(solution)/shard_map/concatenate | solution.py:337
  25.2 1.6 %collective-permute-start.4 = (bf16[64,2176]{1,0:T(8,128)(2,1)S(1)}, bf16[64,2176]{1,0:T(8,128)(2,1)S(1)}, u32[]{:S(2)}, u32[]{:S(2)}) collective-permute-start(bf16[64,2176]{1,0:T(8,128)(2,1)S(1)} %pad_maximum_fusion.2), channel_id=1, source_target_pairs={{0,4},{1,5},{2,6},{3,7},{4,0},{5,1},{6,2},{7,3},{8,12},{9,13},{10,... | collective-permute-start | bytes 835592 | tf_op jit(solution)/shard_map/ppermute | solution.py:289
  26.8 5.7 %collective-permute-done.4 = bf16[64,2176]{1,0:T(8,128)(2,1)S(1)} collective-permute-done((bf16[64,2176]{1,0:T(8,128)(2,1)S(1)}, bf16[64,2176]{1,0:T(8,128)(2,1)S(1)}, u32[]{:S(2)}, u32[]{:S(2)}) %collective-permute-start.4) | collective-permute-done | bytes 278560 | tf_op jit(solution)/shard_map/ppermute | solution.py:289
  32.5 0.1 collective-permute-start.5
  32.6 0.1 pad_maximum_fusion.1
  32.7 0.9 %collective-permute-start.6 = (bf16[1024,256]{1,0:T(8,128)(2,1)S(1)}, bf16[1024,256]{1,0:T(8,128)(2,1)S(1)}, u32[]{:S(2)}, u32[]{:S(2)}) collective-permute-start(bf16[1024,256]{1,0:T(8,128)(2,1)S(1)} %pad_maximum_fusion.1), channel_id=1, source_target_pairs={{0,1},{1,0},{2,3},{3,2},{4,5},{5,4},{6,7},{7,6},{8,9},{9,8},{10,11... | collective-permute-start | bytes 1572872 | tf_op jit(solution)/shard_map/ppermute | solution.py:289
  33.5 1.2 %collective-permute-start.7 = (bf16[128,1024]{1,0:T(8,128)(2,1)S(1)}, bf16[128,1024]{1,0:T(8,128)(2,1)S(1)}, u32[]{:S(2)}, u32[]{:S(2)}) collective-permute-start(bf16[128,1024]{1,0:T(8,128)(2,1)S(1)} %get-tuple-element.14), channel_id=1, source_target_pairs={{0,1},{1,0},{2,3},{3,2},{4,5},{5,4},{6,7},{7,6},{8,9},{9,8},{10,11... | collective-permute-start | bytes 786440 | tf_op jit(solution)/shard_map/ppermute | solution.py:289
  34.8 0.8 %pad_maximum_fusion.refs_5_ = bf16[1024,256]{1,0:T(8,128)(2,1)} fusion(bf16[1024,128]{1,0:T(8,128)(2,1)S(1)} %get-tuple-element.27, bf16[1024,128]{1,0:T(8,128)(2,1)S(1)} %get-tuple-element.33), kind=kLoop, calls=%fused_computation.1 | loop fusion | flops 1048576 | bytes 1048576 | tf_op jit(solution)/shard_map/concatenate | solution.py:317
  35.6 17.1 %collective-permute-done.7.refs_8_ = bf16[128,1024]{1,0:T(8,128)(2,1)S(1)} collective-permute-done((bf16[128,1024]{1,0:T(8,128)(2,1)S(1)}, bf16[128,1024]{1,0:T(8,128)(2,1)S(1)}, u32[]{:S(2)}, u32[]{:S(2)}) %collective-permute-start.7) | collective-permute-done | bytes 262176 | tf_op jit(solution)/shard_map/ppermute | solution.py:289
  52.7 0.7 copy-done.6
  53.4 0.2 copy-done.2
  53.6 0.2 copy-done.1
  53.8 6.0 %branches.1 = (bf16[2,128,1024]{2,1,0:T(8,128)(2,1)}, bf16[2,128,1024]{2,1,0:T(8,128)(2,1)}) custom-call(bf16[128,2176]{1,0:T(8,128)(2,1)} %copy-done, bf16[128,2176]{1,0:T(8,128)(2,1)} %copy-done.1, bf16[1,2048,256]{2,1,0:T(8,128)(2,1)} %refs_2_.1, bf16[1,2048,256]{2,1,0:T(8,128)(2,1)} %refs_3_.1, bf16[1,256,2048]{2,1,0:T(8,128)(2,1)} %refs_4_.1, ...), custom_call_target="tpu_custom_call" | custom-call | tf_op jit(solution)/shard_map/branches/pallas_call | solution.py:233
  59.8 0.1 collective-permute-start.8
  59.9 2.1 %collective-permute-done.8 = bf16[2,128,1024]{2,1,0:T(8,128)(2,1)S(1)} collective-permute-done((bf16[2,128,1024]{2,1,0:T(8,128)(2,1)}, bf16[2,128,1024]{2,1,0:T(8,128)(2,1)S(1)}, u32[]{:S(2)}, u32[]{:S(2)}) %collective-permute-start.8) | collective-permute-done | bytes 524320 | tf_op jit(solution)/shard_map/ppermute | solution.py:289
  62.0 1.2 %convert_add_fusion = f32[2,128,1024]{2,1,0:T(8,128)S(1)} fusion(bf16[2,128,1024]{2,1,0:T(8,128)(2,1)S(1)} %collective-permute-done.8, bf16[2,128,1024]{2,1,0:T(8,128)(2,1)} %get-tuple-element.15), kind=kLoop, calls=%fused_computation | loop fusion | flops 786432 | bytes 2097152 | tf_op jit(solution)/shard_map/add | solution.py:349
  63.2 0.1 convert_element_type.43
  63.3 1.6 %collective-permute-start.9 = (bf16[64,1024]{1,0:T(8,128)(2,1)S(1)}, bf16[64,1024]{1,0:T(8,128)(2,1)S(1)}, u32[]{:S(2)}, u32[]{:S(2)}) collective-permute-start(bf16[64,1024]{1,0:T(8,128)(2,1)S(1)} %get-tuple-element.19), channel_id=1, source_target_pairs={{0,4},{1,5},{2,6},{3,7},{4,0},{5,1},{6,2},{7,3},{8,12},{9,13},{10,... | collective-permute-start | bytes 393224 | tf_op jit(solution)/shard_map/ppermute | solution.py:289
  64.9 0.7 collective-permute-start.11
  65.7 1.2 %collective-permute-start.10 = (bf16[64,1024]{1,0:T(8,128)(2,1)S(1)}, bf16[64,1024]{1,0:T(8,128)(2,1)S(1)}, u32[]{:S(2)}, u32[]{:S(2)}) collective-permute-start(bf16[64,1024]{1,0:T(8,128)(2,1)S(1)} %get-tuple-element.21), channel_id=1, source_target_pairs={{0,1},{1,0},{2,3},{3,2},{4,5},{5,4},{6,7},{7,6},{8,9},{9,8},{10,11... | collective-permute-start | bytes 393224 | tf_op jit(solution)/shard_map/ppermute | solution.py:289
  66.9 4.4 %collective-permute-done.9 = bf16[64,1024]{1,0:T(8,128)(2,1)S(1)} collective-permute-done((bf16[64,1024]{1,0:T(8,128)(2,1)S(1)}, bf16[64,1024]{1,0:T(8,128)(2,1)S(1)}, u32[]{:S(2)}, u32[]{:S(2)}) %collective-permute-start.9) | collective-permute-done | bytes 131104 | tf_op jit(solution)/shard_map/ppermute | solution.py:289
  71.3 0.9 %collective-permute-done.11 = bf16[64,1024]{1,0:T(8,128)(2,1)S(1)} collective-permute-done((bf16[64,1024]{1,0:T(8,128)(2,1)S(1)}, bf16[64,1024]{1,0:T(8,128)(2,1)S(1)}, u32[]{:S(2)}, u32[]{:S(2)}) %collective-permute-start.11) | collective-permute-done | bytes 131104 | tf_op jit(solution)/shard_map/ppermute | solution.py:289
  72.2 0.8 collective-permute-done.10
  73.0 0.1 fusion.13
  73.1 1.2 %collective-permute-start.12 = (bf16[16,1024]{1,0:T(8,128)(2,1)S(1)}, bf16[16,1024]{1,0:T(8,128)(2,1)S(1)}, u32[]{:S(2)}, u32[]{:S(2)}) collective-permute-start(bf16[16,1024]{1,0:T(8,128)(2,1)S(1)} %get-tuple-element.28), channel_id=1, source_target_pairs={{0,24},{1,25},{2,26},{3,27},{4,28},{5,29},{6,30},{7,31},{8,0},{9,1... | collective-permute-start | bytes 98312 | tf_op jit(solution)/shard_map/ppermute | solution.py:289
  74.3 0.9 %collective-permute-start.14 = (bf16[16,1024]{1,0:T(8,128)(2,1)S(1)}, bf16[16,1024]{1,0:T(8,128)(2,1)S(1)}, u32[]{:S(2)}, u32[]{:S(2)}) collective-permute-start(bf16[16,1024]{1,0:T(8,128)(2,1)S(1)} %get-tuple-element.29), channel_id=1, source_target_pairs={{0,8},{1,9},{2,10},{3,11},{4,12},{5,13},{6,14},{7,15},{8,16},{9,17... | collective-permute-start | bytes 98312 | tf_op jit(solution)/shard_map/ppermute | solution.py:289
  75.2 2.1 %collective-permute-start.13 = (bf16[16,1024]{1,0:T(8,128)(2,1)S(1)}, bf16[16,1024]{1,0:T(8,128)(2,1)S(1)}, u32[]{:S(2)}, u32[]{:S(2)}) collective-permute-start(bf16[16,1024]{1,0:T(8,128)(2,1)S(1)} %get-tuple-element.30), channel_id=1, source_target_pairs={{0,16},{1,17},{2,18},{3,19},{4,20},{5,21},{6,22},{7,23},{8,24},{9,... | collective-permute-start | bytes 98312 | tf_op jit(solution)/shard_map/ppermute | solution.py:289
  77.2 2.8 %collective-permute-done.14 = bf16[16,1024]{1,0:T(8,128)(2,1)S(1)} collective-permute-done((bf16[16,1024]{1,0:T(8,128)(2,1)S(1)}, bf16[16,1024]{1,0:T(8,128)(2,1)S(1)}, u32[]{:S(2)}, u32[]{:S(2)}) %collective-permute-start.14) | collective-permute-done | bytes 32800 | tf_op jit(solution)/shard_map/ppermute | solution.py:289
  80.1 0.6 collective-permute-done.13
  80.7 0.6 fusion.6
  (32 shorter events, 0.2 us)
Async XLA Ops:
  0.0 8.9 %copy-start.9 = (f32[16,6]{0,1:T(8,128)S(1)}, f32[16,6]{0,1:T(8,128)}, u32[]{:S(2)}) copy-start(f32[16,6]{0,1:T(8,128)} %param.33) | copy-start | bytes 1156
  0.0 9.0 %copy-start.11 = (s32[16,6]{0,1:T(8,128)S(1)}, s32[16,6]{0,1:T(8,128)}, u32[]{:S(2)}) copy-start(s32[16,6]{0,1:T(8,128)} %param.32) | copy-start | bytes 1156
  0.0 9.2 %copy-start.10 = (bf16[2048]{0:T(1024)(128)(2,1)S(1)}, bf16[2048]{0:T(1024)(128)(2,1)}, u32[]{:S(2)}) copy-start(bf16[2048]{0:T(1024)(128)(2,1)} %param.28) | copy-start | bytes 12292
  0.0 9.8 %copy-start.3 = (bf16[256,1024]{1,0:T(8,128)(2,1)S(1)}, bf16[256,1024]{1,0:T(8,128)(2,1)}, u32[]{:S(2)}) copy-start(bf16[256,1024]{1,0:T(8,128)(2,1)} %param.31) | copy-start | bytes 1572868
  0.0 10.6 %copy-start.4 = (bf16[1024,256]{1,0:T(8,128)(2,1)S(1)}, bf16[1024,256]{1,0:T(8,128)(2,1)}, u32[]{:S(2)}) copy-start(bf16[1024,256]{1,0:T(8,128)(2,1)} %param.30) | copy-start | bytes 1572868
  0.0 10.6 %copy-start.5 = (bf16[1024,256]{1,0:T(8,128)(2,1)S(1)}, bf16[1024,256]{1,0:T(8,128)(2,1)}, u32[]{:S(2)}) copy-start(bf16[1024,256]{1,0:T(8,128)(2,1)} %param.29) | copy-start | bytes 1572868
  5.9 5.6 %collective-permute-start = (bf16[16,2048]{1,0:T(8,128)(2,1)}, bf16[16,2048]{1,0:T(8,128)(2,1)S(1)}, u32[]{:S(2)}, u32[]{:S(2)}) collective-permute-start(bf16[16,2048]{1,0:T(8,128)(2,1)} %mixer.1.refs_4_), channel_id=1, source_target_pairs={{0,1},{1,0},{2,3},{3,2},{4,5},{5,4},{6,7},{7,6},{8,9},{9,8},{10,11... | collective-permute-start | bytes 196616 | tf_op jit(solution)/shard_map/ppermute | solution.py:289
  11.5 0.6 copy-start.7
  13.9 6.6 %collective-permute-start.3 = (bf16[16,2176]{1,0:T(8,128)(2,1)}, bf16[16,2176]{1,0:T(8,128)(2,1)S(1)}, u32[]{:S(2)}, u32[]{:S(2)}) collective-permute-start(bf16[16,2176]{1,0:T(8,128)(2,1)} %get-tuple-element.12), channel_id=1, source_target_pairs={{0,24},{1,25},{2,26},{3,27},{4,28},{5,29},{6,30},{7,31},{8,0},{9,1... | collective-permute-start | bytes 208904 | tf_op jit(solution)/shard_map/ppermute | solution.py:289
  18.0 5.5 %collective-permute-start.2 = (bf16[16,2176]{1,0:T(8,128)(2,1)}, bf16[16,2176]{1,0:T(8,128)(2,1)S(1)}, u32[]{:S(2)}, u32[]{:S(2)}) collective-permute-start(bf16[16,2176]{1,0:T(8,128)(2,1)} %get-tuple-element.12), channel_id=1, source_target_pairs={{0,16},{1,17},{2,18},{3,19},{4,20},{5,21},{6,22},{7,23},{8,24},{9,... | collective-permute-start | bytes 208904 | tf_op jit(solution)/shard_map/ppermute | solution.py:289
  18.0 6.3 %collective-permute-start.1 = (bf16[16,2176]{1,0:T(8,128)(2,1)}, bf16[16,2176]{1,0:T(8,128)(2,1)S(1)}, u32[]{:S(2)}, u32[]{:S(2)}) collective-permute-start(bf16[16,2176]{1,0:T(8,128)(2,1)} %get-tuple-element.12), channel_id=1, source_target_pairs={{0,8},{1,9},{2,10},{3,11},{4,12},{5,13},{6,14},{7,15},{8,16},{9,17... | collective-permute-start | bytes 208904 | tf_op jit(solution)/shard_map/ppermute | solution.py:289
  25.2 7.3 %collective-permute-start.4 = (bf16[64,2176]{1,0:T(8,128)(2,1)S(1)}, bf16[64,2176]{1,0:T(8,128)(2,1)S(1)}, u32[]{:S(2)}, u32[]{:S(2)}) collective-permute-start(bf16[64,2176]{1,0:T(8,128)(2,1)S(1)} %pad_maximum_fusion.2), channel_id=1, source_target_pairs={{0,4},{1,5},{2,6},{3,7},{4,0},{5,1},{6,2},{7,3},{8,12},{9,13},{10,... | collective-permute-start | bytes 835592 | tf_op jit(solution)/shard_map/ppermute | solution.py:289
  32.5 20.2 %copy-start = (bf16[128,2176]{1,0:T(8,128)(2,1)}, bf16[128,2176]{1,0:T(8,128)(2,1)S(1)}, u32[]{:S(2)}) copy-start(bf16[128,2176]{1,0:T(8,128)(2,1)S(1)} %constant_dynamic-update-slice_fusion.refs_0_) | copy-start | bytes 1671172
  32.5 20.2 %collective-permute-start.5 = (bf16[128,2176]{1,0:T(8,128)(2,1)S(1)}, bf16[128,2176]{1,0:T(8,128)(2,1)S(1)}, u32[]{:S(2)}, u32[]{:S(2)}) collective-permute-start(bf16[128,2176]{1,0:T(8,128)(2,1)S(1)} %constant_dynamic-update-slice_fusion.refs_0_), channel_id=1, source_target_pairs={{0,2},{1,3},{2,0},{3,1},{4,6},{5,7},{6,4},{7,5},{8,10},{9,11},{10,... | collective-permute-start | bytes 1671176 | tf_op jit(solution)/shard_map/ppermute | solution.py:289
  32.7 20.0 %collective-permute-start.6 = (bf16[1024,256]{1,0:T(8,128)(2,1)S(1)}, bf16[1024,256]{1,0:T(8,128)(2,1)S(1)}, u32[]{:S(2)}, u32[]{:S(2)}) collective-permute-start(bf16[1024,256]{1,0:T(8,128)(2,1)S(1)} %pad_maximum_fusion.1), channel_id=1, source_target_pairs={{0,1},{1,0},{2,3},{3,2},{4,5},{5,4},{6,7},{7,6},{8,9},{9,8},{10,11... | collective-permute-start | bytes 1572872 | tf_op jit(solution)/shard_map/ppermute | solution.py:289
  33.5 19.1 %collective-permute-start.7 = (bf16[128,1024]{1,0:T(8,128)(2,1)S(1)}, bf16[128,1024]{1,0:T(8,128)(2,1)S(1)}, u32[]{:S(2)}, u32[]{:S(2)}) collective-permute-start(bf16[128,1024]{1,0:T(8,128)(2,1)S(1)} %get-tuple-element.14), channel_id=1, source_target_pairs={{0,1},{1,0},{2,3},{3,2},{4,5},{5,4},{6,7},{7,6},{8,9},{9,8},{10,11... | collective-permute-start | bytes 786440 | tf_op jit(solution)/shard_map/ppermute | solution.py:289
  52.7 0.7 copy-start.6
  52.7 0.9 %copy-start.2 = (bf16[1024,256]{1,0:T(8,128)(2,1)}, bf16[1024,256]{1,0:T(8,128)(2,1)S(1)}, u32[]{:S(2)}) copy-start(bf16[1024,256]{1,0:T(8,128)(2,1)S(1)} %collective-permute-done.6.refs_6_) | copy-start | bytes 1572868
  52.7 1.1 %copy-start.1 = (bf16[128,2176]{1,0:T(8,128)(2,1)}, bf16[128,2176]{1,0:T(8,128)(2,1)S(1)}, u32[]{:S(2)}) copy-start(bf16[128,2176]{1,0:T(8,128)(2,1)S(1)} %collective-permute-done.5.refs_1_) | copy-start | bytes 1671172
  59.8 2.2 %collective-permute-start.8 = (bf16[2,128,1024]{2,1,0:T(8,128)(2,1)}, bf16[2,128,1024]{2,1,0:T(8,128)(2,1)S(1)}, u32[]{:S(2)}, u32[]{:S(2)}) collective-permute-start(bf16[2,128,1024]{2,1,0:T(8,128)(2,1)} %get-tuple-element.16), channel_id=1, source_target_pairs={{0,2},{1,3},{2,0},{3,1},{4,6},{5,7},{6,4},{7,5},{8,10},{9,11},{10,... | collective-permute-start | bytes 1572872 | tf_op jit(solution)/shard_map/ppermute | solution.py:289
  63.2 17.5 %copy-start.8 = (f32[16,2048]{1,0:T(8,128)S(1)}, f32[16,2048]{1,0:T(8,128)}, u32[]{:S(2)}) copy-start(f32[16,2048]{1,0:T(8,128)} %get-tuple-element.11) | copy-start | bytes 393220
  63.3 8.0 %collective-permute-start.9 = (bf16[64,1024]{1,0:T(8,128)(2,1)S(1)}, bf16[64,1024]{1,0:T(8,128)(2,1)S(1)}, u32[]{:S(2)}, u32[]{:S(2)}) collective-permute-start(bf16[64,1024]{1,0:T(8,128)(2,1)S(1)} %get-tuple-element.19), channel_id=1, source_target_pairs={{0,4},{1,5},{2,6},{3,7},{4,0},{5,1},{6,2},{7,3},{8,12},{9,13},{10,... | collective-permute-start | bytes 393224 | tf_op jit(solution)/shard_map/ppermute | solution.py:289
  64.9 7.3 %collective-permute-start.11 = (bf16[64,1024]{1,0:T(8,128)(2,1)S(1)}, bf16[64,1024]{1,0:T(8,128)(2,1)S(1)}, u32[]{:S(2)}, u32[]{:S(2)}) collective-permute-start(bf16[64,1024]{1,0:T(8,128)(2,1)S(1)} %get-tuple-element.20), channel_id=1, source_target_pairs={{0,5},{1,4},{2,7},{3,6},{4,1},{5,0},{6,3},{7,2},{8,13},{9,12},{10,... | collective-permute-start | bytes 393224 | tf_op jit(solution)/shard_map/ppermute | solution.py:289
  65.7 7.3 %collective-permute-start.10 = (bf16[64,1024]{1,0:T(8,128)(2,1)S(1)}, bf16[64,1024]{1,0:T(8,128)(2,1)S(1)}, u32[]{:S(2)}, u32[]{:S(2)}) collective-permute-start(bf16[64,1024]{1,0:T(8,128)(2,1)S(1)} %get-tuple-element.21), channel_id=1, source_target_pairs={{0,1},{1,0},{2,3},{3,2},{4,5},{5,4},{6,7},{7,6},{8,9},{9,8},{10,11... | collective-permute-start | bytes 393224 | tf_op jit(solution)/shard_map/ppermute | solution.py:289
  73.1 4.2 %collective-permute-start.12 = (bf16[16,1024]{1,0:T(8,128)(2,1)S(1)}, bf16[16,1024]{1,0:T(8,128)(2,1)S(1)}, u32[]{:S(2)}, u32[]{:S(2)}) collective-permute-start(bf16[16,1024]{1,0:T(8,128)(2,1)S(1)} %get-tuple-element.28), channel_id=1, source_target_pairs={{0,24},{1,25},{2,26},{3,27},{4,28},{5,29},{6,30},{7,31},{8,0},{9,1... | collective-permute-start | bytes 98312 | tf_op jit(solution)/shard_map/ppermute | solution.py:289
  74.3 5.8 %collective-permute-start.14 = (bf16[16,1024]{1,0:T(8,128)(2,1)S(1)}, bf16[16,1024]{1,0:T(8,128)(2,1)S(1)}, u32[]{:S(2)}, u32[]{:S(2)}) collective-permute-start(bf16[16,1024]{1,0:T(8,128)(2,1)S(1)} %get-tuple-element.29), channel_id=1, source_target_pairs={{0,8},{1,9},{2,10},{3,11},{4,12},{5,13},{6,14},{7,15},{8,16},{9,17... | collective-permute-start | bytes 98312 | tf_op jit(solution)/shard_map/ppermute | solution.py:289
  75.2 5.5 %collective-permute-start.13 = (bf16[16,1024]{1,0:T(8,128)(2,1)S(1)}, bf16[16,1024]{1,0:T(8,128)(2,1)S(1)}, u32[]{:S(2)}, u32[]{:S(2)}) collective-permute-start(bf16[16,1024]{1,0:T(8,128)(2,1)S(1)} %get-tuple-element.30), channel_id=1, source_target_pairs={{0,16},{1,17},{2,18},{3,19},{4,20},{5,21},{6,22},{7,23},{8,24},{9,... | collective-permute-start | bytes 98312 | tf_op jit(solution)/shard_map/ppermute | solution.py:289
where the time goes:
time: 81.7 us; the launch traced here: 81.3 us
  waiting for transfers between devices  38.8 us (47%)
  starting transfers between devices  19.7 us (24%)
  Pallas kernels  13.7 us (17%)
  other arithmetic  4.56 us (6%)
  local copies, waits for them, and re-layouts  4.46 us (5%)
    ppermute x15, waiting for transfers between devices, send(): return lax.ppermute(x, ('ep', 'tp'), pairs)  38.8 us
    ppermute x15, starting transfers between devices, send(): return lax.ppermute(x, ('ep', 'tp'), pairs)  19.7 us
    pallas_call x1, Pallas kernels, branches(): pl.pallas_call(lambda *refs: branch_kernel(tp_count, fanout, *refs), out_...  6 us
    pallas_call x1, Pallas kernels, mixer(): pl.pallas_call(mixer_kernel, out_shape=jax.ShapeDtypeStruct(tokens.shape,...  5.86 us
    unnamed x29, local copies, waits for them, and re-layouts  2.77 us
    pallas_call x1, Pallas kernels, norm_rows(): pl.pallas_call(lambda *refs: norm_kernel(fanout, *refs), out_shape=(jax.S...  1.81 us
  transfers between devices with their start and end apart: 15, of which 11 were waited for; matrix products, arithmetic and copies ran while one was open for 5% of the time, Pallas kernels for 0%

commit v1 on v0

--- a/solution.py
+++ b/solution.py
@@ -134,30 +134,20 @@
         ),
         in_specs=[vmem] * (4 + len(parts)),
         out_specs=(vmem, vmem),
+        compiler_params=pltpu.CompilerParams(vmem_limit_bytes=8 * 1024 * 1024),
         name="norm",
-    )(tokens, gain, gate, meta, *parts)
+    )(in_vmem(tokens), gain, gate, meta, *[in_vmem(part) for part in parts])
 
 
 def silu(v):
     return v / (1.0 + jnp.exp(-v))
 
 
-def branch_kernel(tp_count, fanout, near, far, eg, eu, ed, *refs):
+def branch_kernel(tp_count, fanout, src, eg, eu, ed, *refs):
     pieces = refs[: 2 * tp_count]
-    near_out, far_out = refs[2 * tp_count : 2 * tp_count + 2]
-    bufs = refs[2 * tp_count + 2 : -1]
-    sems = refs[-1]
-    sources = [eg, eu, *pieces[:tp_count], ed, *pieces[tp_count:]]
-    copies = [
-        pltpu.make_async_copy(src, dst, sems.at[i])
-        for i, (src, dst) in enumerate(zip(sources, bufs))
-    ]
-    for copy in copies:
-        copy.start()
-    eg_buf, eu_buf = bufs[0], bufs[1]
-    dg_bufs = bufs[2 : 2 + tp_count]
-    ed_buf = bufs[2 + tp_count]
-    dd_bufs = bufs[3 + tp_count :]
+    dst = refs[2 * tp_count]
+    eg_buf, eu_buf, ed_buf = eg, eu, ed
+    dg_bufs, dd_bufs = pieces[:tp_count], pieces[tp_count:]
     width = eg_buf.shape[1]
     block = width // tp_count
     units = dd_bufs[0].shape[0]
@@ -166,18 +156,10 @@
     tp_index = lax.axis_index("tp")
     spots = [lax.rem(tp_index - t + tp_count, tp_count) * block for t in range(tp_count)]
     spots = [pl.multiple_of(s, LANES) for s in spots]
-    rows = near.shape[0]
+    rows = src.shape[0]
     step = min(rows, 256)
-    held = list(copies)
-
-    def need(count):
-        while len(copies) - len(held) < count:
-            held.pop(0).wait()
-
-    if rows != step:
-        need(len(copies))
-
-    def work(src, dst, start):
+
+    def work(start):
         at = pl.ds(start, step)
         info = src[at, width:].astype(F32)
         lane = lax.broadcasted_iota(jnp.int32, info.shape, 1)
@@ -195,51 +177,46 @@
             weight = jnp.sum(
                 jnp.where((lane < fanout) & (info == own), high + low, 0.0), axis=1, keepdims=True
             )
-            need(1)
             gate = dot(x, eg_buf[k])
-            need(2)
             hidden.append((silu(gate) * dot(x, eu_buf[k]) * weight).astype(BF16))
-        need(2 + tp_count)
         both = dot(src[at, pl.ds(spots[0], block)], dg_bufs[0][...])
         for t in range(1, tp_count):
             both = both + dot(src[at, pl.ds(spots[t], block)], dg_bufs[t][...])
         dense = (silu(both[:, :units]) * both[:, units:] * branch).astype(BF16)
-        need(len(copies))
         for t in range(tp_count):
             total = dot(dense, dd_bufs[t][...])
             for k in range(per_device):
                 total = total + dot(hidden[k], ed_buf[k, :, pl.ds(spots[t], block)])
             dst[t, at, :] = total.astype(BF16)
 
-    for src, dst in ((far, far_out), (near, near_out)):
-        if rows == step:
-            work(src, dst, 0)
-        else:
-
-            def body(i, carry, src=src, dst=dst):
-                work(src, dst, pl.multiple_of(i * step, step))
-                return carry
-
-            lax.fori_loop(0, rows // step, body, 0)
-
-
-def branches(fanout, near, far, eg, eu, ed, gate_pieces, down_pieces):
+    if rows == step:
+        work(0)
+    else:
+
+        def body(i, carry):
+            work(pl.multiple_of(i * step, step))
+            return carry
+
+        lax.fori_loop(0, rows // step, body, 0)
+
+
+def in_vmem(a):
+    return pltpu.with_memory_space_constraint(a, pltpu.VMEM)
+
+
+def branches(fanout, rows, eg, eu, ed, gate_pieces, down_pieces):
     vmem = pl.BlockSpec(memory_space=pltpu.VMEM)
-    hbm = pl.BlockSpec(memory_space=pl.ANY)
     tp_count = len(gate_pieces)
-    width = eg.shape[1]
-    shape = jax.ShapeDtypeStruct((tp_count, near.shape[0], width // tp_count), BF16)
-    order = [eg, eu, *gate_pieces, ed, *down_pieces]
+    shape = (tp_count, rows.shape[0], eg.shape[1] // tp_count)
+    args = [in_vmem(a) for a in (rows, eg, eu, ed, *gate_pieces, *down_pieces)]
     return pl.pallas_call(
         lambda *refs: branch_kernel(tp_count, fanout, *refs),
-        out_shape=(shape, shape),
-        in_specs=[vmem, vmem]
-        + [hbm] * (3 + 2 * tp_count),
-        out_specs=(vmem, vmem),
-        scratch_shapes=[pltpu.VMEM(a.shape, a.dtype) for a in order]
-        + [pltpu.SemaphoreType.DMA((len(order),))],
+        out_shape=jax.ShapeDtypeStruct(shape, BF16),
+        in_specs=[vmem] * len(args),
+        out_specs=vmem,
+        compiler_params=pltpu.CompilerParams(vmem_limit_bytes=24 * 1024 * 1024),
         name="branches",
-    )(near, far, eg, eu, ed, *gate_pieces, *down_pieces)
+    )(*args)
 
 
 def on_device(
@@ -336,29 +313,37 @@
 
     rows = jnp.concatenate([payload] + [send(payload, dz=s) for s in range(1, z_count)], axis=0)
     rows = jnp.concatenate([rows] + [send(rows, dy=s) for s in range(1, y_count)], axis=0)
+    weights = (expert_gate, expert_up, expert_down, gate_pieces, down_pieces)
+    near_sum = branches(fanout, rows, *weights)
     if cores == 2:
         far = send(rows, dc=1)
-    else:
-        far = rows
-    near_sum, far_sum = branches(
-        fanout, rows, far, expert_gate, expert_up, expert_down, gate_pieces, down_pieces
-    )
-
-    total = near_sum.astype(F32)
-    if cores == 2:
-        total = total + send(far_sum, dc=1).astype(F32)
-    total = total.reshape(tp_count, y_count, z_count * sequences, block)
-    narrow = total.astype(BF16)
-    summed = total[0, 0]
-    for t in range(tp_count):
-        for y in range(y_count):
-            if (t, y) != (0, 0):
-                summed = summed + send(narrow[t, y], dx=-t, dy=-y).astype(F32)
-    summed = summed.reshape(z_count, sequences, block)
-    narrow = summed.astype(BF16)
-    result = lax.dynamic_slice_in_dim(after_mix, tp_index * block, block, 1) + summed[0]
+        back = send(branches(fanout, far, *weights), dc=1)
+
+    reach = z_count * sequences
+
+    def chip_sum(t, y):
+        at = slice(y * reach, (y + 1) * reach)
+        total = near_sum[t, at].astype(F32)
+        if cores == 2:
+            total = total + back[t, at].astype(F32)
+        return total.astype(BF16)
+
+    pieces = [
+        send(chip_sum(t, y), dx=-t, dy=-y) if (t, y) != (0, 0) else chip_sum(t, y)
+        for t in range(tp_count)
+        for y in range(y_count)
+    ]
+
+    def plane_sum(z):
+        at = slice(z * sequences, (z + 1) * sequences)
+        total = pieces[0][at].astype(F32)
+        for piece in pieces[1:]:
+            total = total + piece[at].astype(F32)
+        return total
+
+    result = lax.dynamic_slice_in_dim(after_mix, tp_index * block, block, 1) + plane_sum(0)
     for z in range(1, z_count):
-        result = result + send(narrow[z], dz=-z).astype(F32)
+        result = result + send(plane_sum(z).astype(BF16), dz=-z).astype(F32)
     return result.astype(BF16)
 
 

time: 81.7 us -> 71.8 us (0.88)
  Pallas kernels: 13.7 us -> 8.32 us
  local copies, waits for them, and re-layouts: 4.46 us -> 0.55 us
  other arithmetic: 4.56 us -> 1.22 us
  waiting for transfers between devices: 38.8 us -> 41.4 us
    pallas_call x1 -> x2, Pallas kernels: 6 us -> 2.22 us  [branches(): pl.pallas_call(lambda *refs: branch_kernel(tp_count, fanout, *refs), out_...]
    ppermute x15, waiting for transfers between devices: 38.8 us -> 41.4 us  [send(): return lax.ppermute(x, ('ep', 'tp'), pairs)]
    unnamed x29, local copies, waits for them, and re-layouts: 2.77 us -> 0.18 us
    pallas_call x1, Pallas kernels: 1.81 us -> 0.23 us  [norm_rows(): pl.pallas_call(lambda *refs: norm_kernel(fanout, *refs), out_shape=(jax.S...]
    add x1 -> x0, other arithmetic: 1.21 us -> none  [on_device(): total = total + send(far_sum, dc=1).astype(F32)]
    concatenate x1, other arithmetic: 0.9 us -> 0.03 us  [on_device(): jnp.concatenate([payload] + [send(payload, dz=s) for s in range(1, z_coun...]
  transfers between devices with their start and end apart: 15 -> 15, of which waited for: 11 -> 13; matrix products, arithmetic and copies ran while one was open for 5% -> 1% of each run, Pallas kernels for 0% -> 2%
where the time goes in v1:
time: 71.8 us; the launch traced here: 71.7 us
  waiting for transfers between devices  41.4 us (58%)
  starting transfers between devices  20 us (28%)
  Pallas kernels  8.32 us (12%)
  other arithmetic  1.22 us (2%)
    ppermute x15, waiting for transfers between devices, send(): return lax.ppermute(x, ('ep', 'tp'), pairs)  41.4 us
    ppermute x15, starting transfers between devices, send(): return lax.ppermute(x, ('ep', 'tp'), pairs)  20 us
    pallas_call x1, Pallas kernels, mixer(): pl.pallas_call(mixer_kernel, out_shape=jax.ShapeDtypeStruct(tokens.shape,...  5.87 us
    pallas_call x2, Pallas kernels, branches(): pl.pallas_call(lambda *refs: branch_kernel(tp_count, fanout, *refs), out_...  2.22 us
  transfers between devices with their start and end apart: 15, of which 13 were waited for; matrix products, arithmetic and copies ran while one was open for 1% of the time, Pallas kernels for 2%

profile of v1, /device:TPU:0, one launch (start us, length us, event | category | flops | bytes accessed | tf_op | source)
XLA Modules:
  0.0 71.7 jit_solution(17577514199328027673)
XLA Ops:
  0.0 5.9 %mixer.1.refs_4_ = bf16[16,2048]{1,0:T(8,128)(2,1)} custom-call(bf16[16,2048]{1,0:T(8,128)(2,1)} %refs_0_.1, f32[1,2048]{1,0:T(1,128)} %bitcast.30, s32[1,16]{1,0:T(1,128)} %bitcast.31, f32[1,128]{1,0:T(1,128)} %constant.28.clone.freq, bf16[2048,256]{1,0:T(8,128)(2,1)} %wq.1, bf16[2048,256]{1,0:T(8,128)(2,1)} %wk.1, bf16[2048,256]{1,0:T(8,128)(2,1)} %wv.1, ...), custom_call_target="tpu_custom_call" | custom-call | tf_op jit(solution)/shard_map/mixer/pallas_call | solution.py:93
  5.9 0.0 copy-start.3
  5.9 0.0 copy-start.5
  5.9 3.0 %collective-permute-start = (bf16[16,2048]{1,0:T(8,128)(2,1)}, bf16[16,2048]{1,0:T(8,128)(2,1)S(1)}, u32[]{:S(2)}, u32[]{:S(2)}) collective-permute-start(bf16[16,2048]{1,0:T(8,128)(2,1)} %mixer.1.refs_4_), channel_id=1, source_target_pairs={{0,1},{1,0},{2,3},{3,2},{4,5},{5,4},{6,7},{7,6},{8,9},{9,8},{10,11... | collective-permute-start | bytes 196616 | tf_op jit(solution)/shard_map/ppermute | solution.py:266
  9.0 0.1 copy.23
  9.1 0.1 copy.22
  9.3 0.2 constant_dynamic-slice_fusion.2
  9.5 0.0 copy-start
  9.5 0.0 copy-start.1
  9.5 0.0 copy-start.2
  9.5 0.1 reduce-precision_convert_fusion
  9.6 0.1 fusion.24.refs_3_
  9.7 1.7 %collective-permute-done.refs_5_ = bf16[16,2048]{1,0:T(8,128)(2,1)S(1)} collective-permute-done((bf16[16,2048]{1,0:T(8,128)(2,1)}, bf16[16,2048]{1,0:T(8,128)(2,1)S(1)}, u32[]{:S(2)}, u32[]{:S(2)}) %collective-permute-start) | collective-permute-done | bytes 65568 | tf_op jit(solution)/shard_map/ppermute | solution.py:266
  11.4 0.2 norm.1
  11.7 2.2 %collective-permute-start.1 = (bf16[16,2176]{1,0:T(8,128)(2,1)S(1)}, bf16[16,2176]{1,0:T(8,128)(2,1)S(1)}, u32[]{:S(2)}, u32[]{:S(2)}) collective-permute-start(bf16[16,2176]{1,0:T(8,128)(2,1)S(1)} %get-tuple-element.10), channel_id=1, source_target_pairs={{0,8},{1,9},{2,10},{3,11},{4,12},{5,13},{6,14},{7,15},{8,16},{9,17... | collective-permute-start | bytes 208904 | tf_op jit(solution)/shard_map/ppermute | solution.py:266
  13.8 2.6 %collective-permute-start.2 = (bf16[16,2176]{1,0:T(8,128)(2,1)S(1)}, bf16[16,2176]{1,0:T(8,128)(2,1)S(1)}, u32[]{:S(2)}, u32[]{:S(2)}) collective-permute-start(bf16[16,2176]{1,0:T(8,128)(2,1)S(1)} %get-tuple-element.10), channel_id=1, source_target_pairs={{0,16},{1,17},{2,18},{3,19},{4,20},{5,21},{6,22},{7,23},{8,24},{9,... | collective-permute-start | bytes 208904 | tf_op jit(solution)/shard_map/ppermute | solution.py:266
  16.4 1.3 %collective-permute-start.3 = (bf16[16,2176]{1,0:T(8,128)(2,1)S(1)}, bf16[16,2176]{1,0:T(8,128)(2,1)S(1)}, u32[]{:S(2)}, u32[]{:S(2)}) collective-permute-start(bf16[16,2176]{1,0:T(8,128)(2,1)S(1)} %get-tuple-element.10), channel_id=1, source_target_pairs={{0,24},{1,25},{2,26},{3,27},{4,28},{5,29},{6,30},{7,31},{8,0},{9,1... | collective-permute-start | bytes 208904 | tf_op jit(solution)/shard_map/ppermute | solution.py:266
  17.8 1.1 %collective-permute-done.1 = bf16[16,2176]{1,0:T(8,128)(2,1)S(1)} collective-permute-done((bf16[16,2176]{1,0:T(8,128)(2,1)S(1)}, bf16[16,2176]{1,0:T(8,128)(2,1)S(1)}, u32[]{:S(2)}, u32[]{:S(2)}) %collective-permute-start.1) | collective-permute-done | bytes 69664 | tf_op jit(solution)/shard_map/ppermute | solution.py:266
  18.9 1.8 %collective-permute-done.2 = bf16[16,2176]{1,0:T(8,128)(2,1)S(1)} collective-permute-done((bf16[16,2176]{1,0:T(8,128)(2,1)S(1)}, bf16[16,2176]{1,0:T(8,128)(2,1)S(1)}, u32[]{:S(2)}, u32[]{:S(2)}) %collective-permute-start.2) | collective-permute-done | bytes 69664 | tf_op jit(solution)/shard_map/ppermute | solution.py:266
  20.7 0.4 collective-permute-done.3
  21.2 1.6 %collective-permute-start.4 = (bf16[64,2176]{1,0:T(8,128)(2,1)S(1)}, bf16[64,2176]{1,0:T(8,128)(2,1)S(1)}, u32[]{:S(2)}, u32[]{:S(2)}) collective-permute-start(bf16[64,2176]{1,0:T(8,128)(2,1)S(1)} %pad_maximum_fusion.2), channel_id=1, source_target_pairs={{0,4},{1,5},{2,6},{3,7},{4,0},{5,1},{6,2},{7,3},{8,12},{9,13},{10,... | collective-permute-start | bytes 835592 | tf_op jit(solution)/shard_map/ppermute | solution.py:266
  22.8 4.9 %collective-permute-done.4 = bf16[64,2176]{1,0:T(8,128)(2,1)S(1)} collective-permute-done((bf16[64,2176]{1,0:T(8,128)(2,1)S(1)}, bf16[64,2176]{1,0:T(8,128)(2,1)S(1)}, u32[]{:S(2)}, u32[]{:S(2)}) %collective-permute-start.4) | collective-permute-done | bytes 278560 | tf_op jit(solution)/shard_map/ppermute | solution.py:266
  27.8 0.1 collective-permute-start.7
  27.9 0.1 pad_maximum_fusion.1
  27.9 1.6 %collective-permute-start.5 = (bf16[1024,256]{1,0:T(8,128)(2,1)S(1)}, bf16[1024,256]{1,0:T(8,128)(2,1)S(1)}, u32[]{:S(2)}, u32[]{:S(2)}) collective-permute-start(bf16[1024,256]{1,0:T(8,128)(2,1)S(1)} %pad_maximum_fusion.1), channel_id=1, source_target_pairs={{0,1},{1,0},{2,3},{3,2},{4,5},{5,4},{6,7},{7,6},{8,9},{9,8},{10,11... | collective-permute-start | bytes 1572872 | tf_op jit(solution)/shard_map/ppermute | solution.py:266
  29.6 0.5 collective-permute-start.6
  30.0 0.1 pad_maximum_fusion.refs_4_
  30.1 17.8 %collective-permute-done.6.refs_7_ = bf16[128,1024]{1,0:T(8,128)(2,1)S(1)} collective-permute-done((bf16[128,1024]{1,0:T(8,128)(2,1)S(1)}, bf16[128,1024]{1,0:T(8,128)(2,1)S(1)}, u32[]{:S(2)}, u32[]{:S(2)}) %collective-permute-start.6) | collective-permute-done | bytes 262176 | tf_op jit(solution)/shard_map/ppermute | solution.py:266
  47.9 0.0 collective-permute-done.5.refs_5_
  48.0 1.1 %branches.3 = bf16[2,128,1024]{2,1,0:T(8,128)(2,1)S(1)} custom-call(bf16[128,2176]{1,0:T(8,128)(2,1)S(1)} %collective-permute-done.7.refs_0_, bf16[1,2048,256]{2,1,0:T(8,128)(2,1)S(1)} %copy-done, bf16[1,2048,256]{2,1,0:T(8,128)(2,1)S(1)} %copy-done.1, bf16[1,256,2048]{2,1,0:T(8,128)(2,1)S(1)} %copy-done.2, bf16[1024,256]{1,0:T(8,128)(2,1)S(1)} %pad_maximum_fusion.refs_4_, ...), custom_call_target="tpu_custom_call" | custom-call | tf_op jit(solution)/shard_map/branches/pallas_call | solution.py:212
  49.1 0.1 collective-permute-start.8
  49.2 1.1 %branches.2 = bf16[2,128,1024]{2,1,0:T(8,128)(2,1)S(1)} custom-call(bf16[128,2176]{1,0:T(8,128)(2,1)S(1)} %constant_dynamic-update-slice_fusion.refs_0_, bf16[1,2048,256]{2,1,0:T(8,128)(2,1)S(1)} %copy-done, bf16[1,2048,256]{2,1,0:T(8,128)(2,1)S(1)} %copy-done.1, bf16[1,256,2048]{2,1,0:T(8,128)(2,1)S(1)} %copy-done.2, ...), custom_call_target="tpu_custom_call" | custom-call | tf_op jit(solution)/shard_map/branches/pallas_call | solution.py:212
  50.3 0.8 %collective-permute-done.8 = bf16[2,128,1024]{2,1,0:T(8,128)(2,1)S(1)} collective-permute-done((bf16[2,128,1024]{2,1,0:T(8,128)(2,1)S(1)}, bf16[2,128,1024]{2,1,0:T(8,128)(2,1)S(1)}, u32[]{:S(2)}, u32[]{:S(2)}) %collective-permute-start.8) | collective-permute-done | bytes 524320 | tf_op jit(solution)/shard_map/ppermute | solution.py:266
  51.1 0.2 add_convert_fusion.3
  51.3 1.6 %collective-permute-start.10 = (bf16[64,1024]{1,0:T(8,128)(2,1)S(1)}, bf16[64,1024]{1,0:T(8,128)(2,1)S(1)}, u32[]{:S(2)}, u32[]{:S(2)}) collective-permute-start(bf16[64,1024]{1,0:T(8,128)(2,1)S(1)} %get-tuple-element.15), channel_id=1, source_target_pairs={{0,1},{1,0},{2,3},{3,2},{4,5},{5,4},{6,7},{7,6},{8,9},{9,8},{10,11... | collective-permute-start | bytes 393224 | tf_op jit(solution)/shard_map/ppermute | solution.py:266
  52.9 1.5 %collective-permute-start.11 = (bf16[64,1024]{1,0:T(8,128)(2,1)S(1)}, bf16[64,1024]{1,0:T(8,128)(2,1)S(1)}, u32[]{:S(2)}, u32[]{:S(2)}) collective-permute-start(bf16[64,1024]{1,0:T(8,128)(2,1)S(1)} %get-tuple-element.14), channel_id=1, source_target_pairs={{0,5},{1,4},{2,7},{3,6},{4,1},{5,0},{6,3},{7,2},{8,13},{9,12},{10,... | collective-permute-start | bytes 393224 | tf_op jit(solution)/shard_map/ppermute | solution.py:266
  54.4 0.5 collective-permute-start.9
  54.8 2.6 %collective-permute-done.10 = bf16[64,1024]{1,0:T(8,128)(2,1)S(1)} collective-permute-done((bf16[64,1024]{1,0:T(8,128)(2,1)S(1)}, bf16[64,1024]{1,0:T(8,128)(2,1)S(1)}, u32[]{:S(2)}, u32[]{:S(2)}) %collective-permute-start.10) | collective-permute-done | bytes 131104 | tf_op jit(solution)/shard_map/ppermute | solution.py:266
  57.5 3.3 %collective-permute-done.11 = bf16[64,1024]{1,0:T(8,128)(2,1)S(1)} collective-permute-done((bf16[64,1024]{1,0:T(8,128)(2,1)S(1)}, bf16[64,1024]{1,0:T(8,128)(2,1)S(1)}, u32[]{:S(2)}, u32[]{:S(2)}) %collective-permute-start.11) | collective-permute-done | bytes 131104 | tf_op jit(solution)/shard_map/ppermute | solution.py:266
  60.8 1.4 %collective-permute-done.9 = bf16[64,1024]{1,0:T(8,128)(2,1)S(1)} collective-permute-done((bf16[64,1024]{1,0:T(8,128)(2,1)S(1)}, bf16[64,1024]{1,0:T(8,128)(2,1)S(1)}, u32[]{:S(2)}, u32[]{:S(2)}) %collective-permute-start.9) | collective-permute-done | bytes 131104 | tf_op jit(solution)/shard_map/ppermute | solution.py:266
  62.2 0.1 fusion.11
  62.2 2.8 %collective-permute-start.12 = (bf16[16,1024]{1,0:T(8,128)(2,1)S(1)}, bf16[16,1024]{1,0:T(8,128)(2,1)S(1)}, u32[]{:S(2)}, u32[]{:S(2)}) collective-permute-start(bf16[16,1024]{1,0:T(8,128)(2,1)S(1)} %get-tuple-element.17), channel_id=1, source_target_pairs={{0,24},{1,25},{2,26},{3,27},{4,28},{5,29},{6,30},{7,31},{8,0},{9,1... | collective-permute-start | bytes 98312 | tf_op jit(solution)/shard_map/ppermute | solution.py:266
  65.0 0.3 collective-permute-start.13
  65.3 0.3 collective-permute-start.14
  65.6 1.0 %collective-permute-done.12 = bf16[16,1024]{1,0:T(8,128)(2,1)S(1)} collective-permute-done((bf16[16,1024]{1,0:T(8,128)(2,1)S(1)}, bf16[16,1024]{1,0:T(8,128)(2,1)S(1)}, u32[]{:S(2)}, u32[]{:S(2)}) %collective-permute-start.12) | collective-permute-done | bytes 32800 | tf_op jit(solution)/shard_map/ppermute | solution.py:266
  66.6 3.2 %collective-permute-done.13 = bf16[16,1024]{1,0:T(8,128)(2,1)S(1)} collective-permute-done((bf16[16,1024]{1,0:T(8,128)(2,1)S(1)}, bf16[16,1024]{1,0:T(8,128)(2,1)S(1)}, u32[]{:S(2)}, u32[]{:S(2)}) %collective-permute-start.13) | collective-permute-done | bytes 32800 | tf_op jit(solution)/shard_map/ppermute | solution.py:266
  69.8 1.2 %collective-permute-done.14 = bf16[16,1024]{1,0:T(8,128)(2,1)S(1)} collective-permute-done((bf16[16,1024]{1,0:T(8,128)(2,1)S(1)}, bf16[16,1024]{1,0:T(8,128)(2,1)S(1)}, u32[]{:S(2)}, u32[]{:S(2)}) %collective-permute-start.14) | collective-permute-done | bytes 32800 | tf_op jit(solution)/shard_map/ppermute | solution.py:266
  71.0 0.7 fusion.18
  (30 shorter events, 0.2 us)
Async XLA Ops:
  0.0 9.0 %copy-start.9 = (f32[16,6]{0,1:T(8,128)S(1)}, f32[16,6]{0,1:T(8,128)}, u32[]{:S(2)}) copy-start(f32[16,6]{0,1:T(8,128)} %param.33) | copy-start | bytes 1156
  0.0 9.1 %copy-start.11 = (s32[16,6]{0,1:T(8,128)S(1)}, s32[16,6]{0,1:T(8,128)}, u32[]{:S(2)}) copy-start(s32[16,6]{0,1:T(8,128)} %param.32) | copy-start | bytes 1156
  0.0 9.2 %copy-start.10 = (bf16[2048]{0:T(1024)(128)(2,1)S(1)}, bf16[2048]{0:T(1024)(128)(2,1)}, u32[]{:S(2)}) copy-start(bf16[2048]{0:T(1024)(128)(2,1)} %param.28) | copy-start | bytes 12292
  0.0 9.2 %copy-start.6 = (bf16[256,1024]{1,0:T(8,128)(2,1)S(1)}, bf16[256,1024]{1,0:T(8,128)(2,1)}, u32[]{:S(2)}) copy-start(bf16[256,1024]{1,0:T(8,128)(2,1)} %param.31) | copy-start | bytes 1572868
  0.0 9.3 %copy-start.7 = (bf16[1024,256]{1,0:T(8,128)(2,1)S(1)}, bf16[1024,256]{1,0:T(8,128)(2,1)}, u32[]{:S(2)}) copy-start(bf16[1024,256]{1,0:T(8,128)(2,1)} %param.30) | copy-start | bytes 1572868
  0.0 9.3 %copy-start.8 = (bf16[1024,256]{1,0:T(8,128)(2,1)S(1)}, bf16[1024,256]{1,0:T(8,128)(2,1)}, u32[]{:S(2)}) copy-start(bf16[1024,256]{1,0:T(8,128)(2,1)} %param.29) | copy-start | bytes 1572868
  5.9 5.5 %copy-start.3 = (bf16[16,2048]{1,0:T(8,128)(2,1)S(1)}, bf16[16,2048]{1,0:T(8,128)(2,1)}, u32[]{:S(2)}) copy-start(bf16[16,2048]{1,0:T(8,128)(2,1)} %refs_0_.1) | copy-start | bytes 196612
  5.9 5.5 %copy-start.4 = (bf16[16,2048]{1,0:T(8,128)(2,1)S(1)}, bf16[16,2048]{1,0:T(8,128)(2,1)}, u32[]{:S(2)}) copy-start(bf16[16,2048]{1,0:T(8,128)(2,1)} %mixer.1.refs_4_) | copy-start | bytes 196612
  5.9 5.5 %copy-start.5 = (f32[2048]{0:T(1024)S(1)}, f32[2048]{0:T(1024)}, u32[]{:S(2)}) copy-start(f32[2048]{0:T(1024)} %param.27) | copy-start | bytes 24580
  5.9 5.5 %collective-permute-start = (bf16[16,2048]{1,0:T(8,128)(2,1)}, bf16[16,2048]{1,0:T(8,128)(2,1)S(1)}, u32[]{:S(2)}, u32[]{:S(2)}) collective-permute-start(bf16[16,2048]{1,0:T(8,128)(2,1)} %mixer.1.refs_4_), channel_id=1, source_target_pairs={{0,1},{1,0},{2,3},{3,2},{4,5},{5,4},{6,7},{7,6},{8,9},{9,8},{10,11... | collective-permute-start | bytes 196616 | tf_op jit(solution)/shard_map/ppermute | solution.py:266
  9.5 38.4 %copy-start = (bf16[1,2048,256]{2,1,0:T(8,128)(2,1)S(1)}, bf16[1,2048,256]{2,1,0:T(8,128)(2,1)}, u32[]{:S(2)}) copy-start(bf16[1,2048,256]{2,1,0:T(8,128)(2,1)} %refs_1_.3) | copy-start | bytes 3145732
  9.5 38.4 %copy-start.1 = (bf16[1,2048,256]{2,1,0:T(8,128)(2,1)S(1)}, bf16[1,2048,256]{2,1,0:T(8,128)(2,1)}, u32[]{:S(2)}) copy-start(bf16[1,2048,256]{2,1,0:T(8,128)(2,1)} %refs_2_.3) | copy-start | bytes 3145732
  9.5 38.4 %copy-start.2 = (bf16[1,256,2048]{2,1,0:T(8,128)(2,1)S(1)}, bf16[1,256,2048]{2,1,0:T(8,128)(2,1)}, u32[]{:S(2)}) copy-start(bf16[1,256,2048]{2,1,0:T(8,128)(2,1)} %refs_3_.3) | copy-start | bytes 3145732
  11.7 7.2 %collective-permute-start.1 = (bf16[16,2176]{1,0:T(8,128)(2,1)S(1)}, bf16[16,2176]{1,0:T(8,128)(2,1)S(1)}, u32[]{:S(2)}, u32[]{:S(2)}) collective-permute-start(bf16[16,2176]{1,0:T(8,128)(2,1)S(1)} %get-tuple-element.10), channel_id=1, source_target_pairs={{0,8},{1,9},{2,10},{3,11},{4,12},{5,13},{6,14},{7,15},{8,16},{9,17... | collective-permute-start | bytes 208904 | tf_op jit(solution)/shard_map/ppermute | solution.py:266
  13.8 6.9 %collective-permute-start.2 = (bf16[16,2176]{1,0:T(8,128)(2,1)S(1)}, bf16[16,2176]{1,0:T(8,128)(2,1)S(1)}, u32[]{:S(2)}, u32[]{:S(2)}) collective-permute-start(bf16[16,2176]{1,0:T(8,128)(2,1)S(1)} %get-tuple-element.10), channel_id=1, source_target_pairs={{0,16},{1,17},{2,18},{3,19},{4,20},{5,21},{6,22},{7,23},{8,24},{9,... | collective-permute-start | bytes 208904 | tf_op jit(solution)/shard_map/ppermute | solution.py:266
  16.4 4.7 %collective-permute-start.3 = (bf16[16,2176]{1,0:T(8,128)(2,1)S(1)}, bf16[16,2176]{1,0:T(8,128)(2,1)S(1)}, u32[]{:S(2)}, u32[]{:S(2)}) collective-permute-start(bf16[16,2176]{1,0:T(8,128)(2,1)S(1)} %get-tuple-element.10), channel_id=1, source_target_pairs={{0,24},{1,25},{2,26},{3,27},{4,28},{5,29},{6,30},{7,31},{8,0},{9,1... | collective-permute-start | bytes 208904 | tf_op jit(solution)/shard_map/ppermute | solution.py:266
  21.2 6.6 %collective-permute-start.4 = (bf16[64,2176]{1,0:T(8,128)(2,1)S(1)}, bf16[64,2176]{1,0:T(8,128)(2,1)S(1)}, u32[]{:S(2)}, u32[]{:S(2)}) collective-permute-start(bf16[64,2176]{1,0:T(8,128)(2,1)S(1)} %pad_maximum_fusion.2), channel_id=1, source_target_pairs={{0,4},{1,5},{2,6},{3,7},{4,0},{5,1},{6,2},{7,3},{8,12},{9,13},{10,... | collective-permute-start | bytes 835592 | tf_op jit(solution)/shard_map/ppermute | solution.py:266
  27.8 20.2 %collective-permute-start.7 = (bf16[128,2176]{1,0:T(8,128)(2,1)S(1)}, bf16[128,2176]{1,0:T(8,128)(2,1)S(1)}, u32[]{:S(2)}, u32[]{:S(2)}) collective-permute-start(bf16[128,2176]{1,0:T(8,128)(2,1)S(1)} %constant_dynamic-update-slice_fusion.refs_0_), channel_id=1, source_target_pairs={{0,2},{1,3},{2,0},{3,1},{4,6},{5,7},{6,4},{7,5},{8,10},{9,11},{10,... | collective-permute-start | bytes 1671176 | tf_op jit(solution)/shard_map/ppermute | solution.py:266
  27.9 20.0 %collective-permute-start.5 = (bf16[1024,256]{1,0:T(8,128)(2,1)S(1)}, bf16[1024,256]{1,0:T(8,128)(2,1)S(1)}, u32[]{:S(2)}, u32[]{:S(2)}) collective-permute-start(bf16[1024,256]{1,0:T(8,128)(2,1)S(1)} %pad_maximum_fusion.1), channel_id=1, source_target_pairs={{0,1},{1,0},{2,3},{3,2},{4,5},{5,4},{6,7},{7,6},{8,9},{9,8},{10,11... | collective-permute-start | bytes 1572872 | tf_op jit(solution)/shard_map/ppermute | solution.py:266
  29.6 18.4 %collective-permute-start.6 = (bf16[128,1024]{1,0:T(8,128)(2,1)S(1)}, bf16[128,1024]{1,0:T(8,128)(2,1)S(1)}, u32[]{:S(2)}, u32[]{:S(2)}) collective-permute-start(bf16[128,1024]{1,0:T(8,128)(2,1)S(1)} %get-tuple-element.12), channel_id=1, source_target_pairs={{0,1},{1,0},{2,3},{3,2},{4,5},{5,4},{6,7},{7,6},{8,9},{9,8},{10,11... | collective-permute-start | bytes 786440 | tf_op jit(solution)/shard_map/ppermute | solution.py:266
  49.1 2.0 %collective-permute-start.8 = (bf16[2,128,1024]{2,1,0:T(8,128)(2,1)S(1)}, bf16[2,128,1024]{2,1,0:T(8,128)(2,1)S(1)}, u32[]{:S(2)}, u32[]{:S(2)}) collective-permute-start(bf16[2,128,1024]{2,1,0:T(8,128)(2,1)S(1)} %branches.3), channel_id=1, source_target_pairs={{0,2},{1,3},{2,0},{3,1},{4,6},{5,7},{6,4},{7,5},{8,10},{9,11},{10,... | collective-permute-start | bytes 1572872 | tf_op jit(solution)/shard_map/ppermute | solution.py:266
  51.3 6.2 %collective-permute-start.10 = (bf16[64,1024]{1,0:T(8,128)(2,1)S(1)}, bf16[64,1024]{1,0:T(8,128)(2,1)S(1)}, u32[]{:S(2)}, u32[]{:S(2)}) collective-permute-start(bf16[64,1024]{1,0:T(8,128)(2,1)S(1)} %get-tuple-element.15), channel_id=1, source_target_pairs={{0,1},{1,0},{2,3},{3,2},{4,5},{5,4},{6,7},{7,6},{8,9},{9,8},{10,11... | collective-permute-start | bytes 393224 | tf_op jit(solution)/shard_map/ppermute | solution.py:266
  52.9 7.9 %collective-permute-start.11 = (bf16[64,1024]{1,0:T(8,128)(2,1)S(1)}, bf16[64,1024]{1,0:T(8,128)(2,1)S(1)}, u32[]{:S(2)}, u32[]{:S(2)}) collective-permute-start(bf16[64,1024]{1,0:T(8,128)(2,1)S(1)} %get-tuple-element.14), channel_id=1, source_target_pairs={{0,5},{1,4},{2,7},{3,6},{4,1},{5,0},{6,3},{7,2},{8,13},{9,12},{10,... | collective-permute-start | bytes 393224 | tf_op jit(solution)/shard_map/ppermute | solution.py:266
  54.4 7.8 %collective-permute-start.9 = (bf16[64,1024]{1,0:T(8,128)(2,1)S(1)}, bf16[64,1024]{1,0:T(8,128)(2,1)S(1)}, u32[]{:S(2)}, u32[]{:S(2)}) collective-permute-start(bf16[64,1024]{1,0:T(8,128)(2,1)S(1)} %get-tuple-element.16), channel_id=1, source_target_pairs={{0,4},{1,5},{2,6},{3,7},{4,0},{5,1},{6,2},{7,3},{8,12},{9,13},{10,... | collective-permute-start | bytes 393224 | tf_op jit(solution)/shard_map/ppermute | solution.py:266
  62.2 4.4 %collective-permute-start.12 = (bf16[16,1024]{1,0:T(8,128)(2,1)S(1)}, bf16[16,1024]{1,0:T(8,128)(2,1)S(1)}, u32[]{:S(2)}, u32[]{:S(2)}) collective-permute-start(bf16[16,1024]{1,0:T(8,128)(2,1)S(1)} %get-tuple-element.17), channel_id=1, source_target_pairs={{0,24},{1,25},{2,26},{3,27},{4,28},{5,29},{6,30},{7,31},{8,0},{9,1... | collective-permute-start | bytes 98312 | tf_op jit(solution)/shard_map/ppermute | solution.py:266
  65.0 4.8 %collective-permute-start.13 = (bf16[16,1024]{1,0:T(8,128)(2,1)S(1)}, bf16[16,1024]{1,0:T(8,128)(2,1)S(1)}, u32[]{:S(2)}, u32[]{:S(2)}) collective-permute-start(bf16[16,1024]{1,0:T(8,128)(2,1)S(1)} %get-tuple-element.19), channel_id=1, source_target_pairs={{0,16},{1,17},{2,18},{3,19},{4,20},{5,21},{6,22},{7,23},{8,24},{9,... | collective-permute-start | bytes 98312 | tf_op jit(solution)/shard_map/ppermute | solution.py:266
  65.3 5.7 %collective-permute-start.14 = (bf16[16,1024]{1,0:T(8,128)(2,1)S(1)}, bf16[16,1024]{1,0:T(8,128)(2,1)S(1)}, u32[]{:S(2)}, u32[]{:S(2)}) collective-permute-start(bf16[16,1024]{1,0:T(8,128)(2,1)S(1)} %get-tuple-element.18), channel_id=1, source_target_pairs={{0,8},{1,9},{2,10},{3,11},{4,12},{5,13},{6,14},{7,15},{8,16},{9,17... | collective-permute-start | bytes 98312 | tf_op jit(solution)/shard_map/ppermute | solution.py:266
